TPU v7x, 32 devices: a whole 2x2x4 slice. The times are simulated.
32 devices in a mesh: ep: 8 (over z, core), tp: 4 (over y, x).
Axes of the slice: x: 2, y: 2, z: 4, core: 2. Of those that a mesh axis runs over, the one named last changes fastest.
Arguments:
- q_latent: bfloat16 [1536, 512], P('ep'), may hold values from -6 to 6
- kv_latent: bfloat16 [1536, 256], P('ep'), may hold values from -6 to 6
- rope_key: bfloat16 [1536, 64], P('ep'), may hold values from -900 to 900
- q_gain: float32 [512], replicated, may hold values from 0.1 to 1.9
- kv_gain: float32 [256], replicated, may hold values from 0.1 to 1.9
- w_query: bfloat16 [512, 3072], P(None, 'tp'), may hold values from -0.25 to 0.25
- w_key: bfloat16 [256, 2048], P(None, 'tp'), may hold values from -0.375 to 0.375
- w_value: bfloat16 [256, 2048], P(None, 'tp'), may hold values from -0.375 to 0.375
- w_mix_out: bfloat16 [2048, 2048], P('tp'), may hold values from -0.125 to 0.125
- expert_in: bfloat16 [1024, 2048], P('ep'), may hold values from -6 to 6
- norm_gain: float32 [2048], replicated, may hold values from 0.1 to 1.9
- routes: int32 [1024, 2], P('ep'), may hold values from 0 to 7, all different within a row; in each aligned block of 128 rows (0 to 127, 128 to 255, ...) at most 64 rows name the same one
- route_scores: float32 [1024, 2], P('ep'), may hold values from 0.05 to 1
- w_gate: bfloat16 [8, 2048, 4096], P('ep', None, 'tp'), may hold values from -0.125 to 0.125
- w_up: bfloat16 [8, 2048, 4096], P('ep', None, 'tp'), may hold values from -0.125 to 0.125
- w_down: bfloat16 [8, 4096, 2048], P('ep', 'tp'), may hold values from -0.125 to 0.125
Outputs:
- mixed: bfloat16 [1536, 2048], P(('ep', 'tp'))
- expert_out: bfloat16 [1024, 2048], P('ep', 'tp')
Inputs may be any that keep to these rules, and one draw needn't show every extreme that they name: `routes`: each row names 2 different experts; in the rows of one index of ep no expert is named by more than 64 rows, a bound that some block reaches.
All inputs are finite; a program needn't handle non-finite values.
Results may differ from a plain program's by a relative error of at most 0.03.
The roundings to bfloat16 on the way count: a program that leaves them out, or rounds other values in their place, can miss the bound.
Values may be sent and summed in bfloat16 or wider, within the bound.
No kernel may reach another device: no remote copies, remote signals or barrier semaphores. Data moves between devices by JAX's collectives and lax.ppermute only.
A program may use at most 64 MiB of HBM per device.

v0:
```python
import jax
import jax.numpy as jnp
from jax import lax
from jax.sharding import PartitionSpec as P

NOPE = 128
ROPE = 64
VDIM = 128
eps_norm = 1e-05
rope_base = 10000.0


def rms_scale(values, gain):
    wide = values.astype(jnp.float32)
    return wide * lax.rsqrt(jnp.mean(wide * wide, -1, keepdims=True) + eps_norm) * gain


def rotate(values, cosine, sine):
    first, second = jnp.split(values, 2, axis=-1)
    return jnp.concatenate([first * cosine - second * sine, first * sine + second * cosine], -1)


def angles(positions):
    inverse = rope_base ** (-jnp.arange(0, ROPE, 2).astype(jnp.float32) / ROPE)
    phase = positions[:, None] * inverse[None, :]
    return (jnp.cos(phase), jnp.sin(phase))


def mixer(q_latent, kv_latent, rope_key, q_gain, kv_gain, w_query, w_key, w_value, w_mix_out):
    token_count = q_latent.shape[0]
    head_count = w_key.shape[1] // NOPE
    offset = lax.axis_index("ep") * token_count
    positions = (offset + jnp.arange(token_count, dtype=jnp.int32)).astype(jnp.float32)
    cosine, sine = angles(positions)
    q_normed = rms_scale(q_latent, q_gain).astype(jnp.bfloat16)
    kv_normed = rms_scale(kv_latent, kv_gain).astype(jnp.bfloat16)
    key_turned = rotate(rope_key.astype(jnp.float32), cosine, sine).astype(jnp.bfloat16)
    query = jnp.dot(q_normed, w_query, preferred_element_type=jnp.float32).astype(jnp.bfloat16)
    query = query.reshape(token_count, head_count, NOPE + ROPE)
    q_pass = query[:, :, :NOPE]
    q_turned = rotate(
        query[:, :, NOPE:].astype(jnp.float32), cosine[:, None, :], sine[:, None, :]
    ).astype(jnp.bfloat16)
    factor = (NOPE + ROPE) ** (-0.5)
    peak = jnp.full((head_count, token_count), -jnp.inf, jnp.float32)
    total = jnp.zeros((head_count, token_count), jnp.float32)
    summed = jnp.zeros((token_count, head_count, VDIM), jnp.float32)
    latent = lax.all_gather(kv_normed, "ep", axis=0, tiled=True)
    turned = lax.all_gather(key_turned, "ep", axis=0, tiled=True)
    count = latent.shape[0]
    keys = jnp.dot(latent, w_key, preferred_element_type=jnp.float32).astype(jnp.bfloat16)
    keys = keys.reshape(count, head_count, NOPE)
    values = jnp.dot(latent, w_value, preferred_element_type=jnp.float32).astype(jnp.bfloat16)
    values = values.reshape(count, head_count, VDIM)
    scores = jnp.einsum("qhd,khd->hqk", q_pass, keys, preferred_element_type=jnp.float32)
    scores = (
        scores + jnp.einsum("qhd,kd->hqk", q_turned, turned, preferred_element_type=jnp.float32)
    ) * factor
    fresh = jnp.max(scores, -1)
    fade = jnp.exp(peak - fresh)
    weights = jnp.exp(scores - fresh[:, :, None])
    total = total * fade + jnp.sum(weights, -1)
    update = jnp.einsum(
        "hqk,khd->qhd", weights.astype(jnp.bfloat16), values, preferred_element_type=jnp.float32
    )
    summed = summed * jnp.transpose(fade)[:, :, None] + update
    peak, total, summed = (fresh, total, summed)
    attended = (summed / jnp.transpose(total)[:, :, None]).astype(jnp.bfloat16)
    attended = attended.reshape(token_count, head_count * VDIM)
    return lax.psum_scatter(
        jnp.dot(attended, w_mix_out, preferred_element_type=jnp.float32).astype(jnp.bfloat16),
        "tp",
        scatter_dimension=0,
        tiled=True,
    )


def experts(expert_in, norm_gain, routes, route_scores, w_gate, w_up, w_down):
    token_count, width = expert_in.shape
    choose = routes.shape[1]
    expert_count = lax.axis_size("ep")
    slots = 2 * choose * token_count // expert_count
    wide = expert_in.astype(jnp.float32)
    centered = wide - jnp.mean(wide, -1, keepdims=True)
    normed = (
        centered
        * lax.rsqrt(jnp.mean(centered * centered, -1, keepdims=True) + eps_norm)
        * norm_gain
    ).astype(jnp.bfloat16)
    shares = route_scores / jnp.sum(route_scores, -1, keepdims=True)
    flat_expert = routes.reshape(-1)
    onehot = (flat_expert[:, None] == jnp.arange(expert_count, dtype=jnp.int32)[None, :]).astype(
        jnp.int32
    )
    before = jnp.sum((jnp.cumsum(onehot, 0) - onehot) * onehot, 1)
    target = flat_expert * slots + before
    source = jnp.arange(token_count * choose, dtype=jnp.int32) // choose
    table = jnp.full((expert_count * slots,), token_count, jnp.int32).at[target].set(source)
    padded = jnp.concatenate([normed, jnp.zeros((1, width), jnp.bfloat16)], 0)
    outgoing = padded[table].reshape(expert_count, slots, width)
    gate_weight = w_gate[0]
    up_weight = w_up[0]
    down_weight = w_down[0]
    arrived = lax.all_to_all(outgoing, "ep", split_axis=0, concat_axis=0, tiled=True).reshape(
        expert_count * slots, width
    )
    gate = jnp.dot(arrived, gate_weight, preferred_element_type=jnp.float32)
    up = jnp.dot(arrived, up_weight, preferred_element_type=jnp.float32)
    hidden = (jax.nn.silu(gate) * up).astype(jnp.bfloat16)
    summed = lax.psum_scatter(
        lax.dot_general(
            down_weight, hidden, (((0,), (1,)), ((), ())), preferred_element_type=jnp.float32
        ).astype(jnp.bfloat16),
        "tp",
        scatter_dimension=0,
        tiled=True,
    )
    feature_count = summed.shape[0]
    returned = lax.all_to_all(
        summed.reshape(feature_count, expert_count, slots),
        "ep",
        split_axis=1,
        concat_axis=1,
        tiled=True,
    )
    picked = jnp.take(returned.reshape(feature_count, expert_count * slots), target, axis=1)
    picked = picked.reshape(feature_count, token_count, choose).astype(jnp.float32)
    combined = jnp.sum(picked * shares[None, :, :], -1)
    return jnp.transpose(combined).astype(jnp.bfloat16)


def body(
    q_latent,
    kv_latent,
    rope_key,
    q_gain,
    kv_gain,
    w_query,
    w_key,
    w_value,
    w_mix_out,
    expert_in,
    norm_gain,
    routes,
    route_scores,
    w_gate,
    w_up,
    w_down,
):
    mixed = mixer(
        q_latent, kv_latent, rope_key, q_gain, kv_gain, w_query, w_key, w_value, w_mix_out
    )
    expert_out = experts(expert_in, norm_gain, routes, route_scores, w_gate, w_up, w_down)
    return (mixed, expert_out)


def solution(mesh):
    in_specs = (
        P("ep", None),
        P("ep", None),
        P("ep", None),
        P(),
        P(),
        P(None, "tp"),
        P(None, "tp"),
        P(None, "tp"),
        P("tp", None),
        P("ep", None),
        P(),
        P("ep", None),
        P("ep", None),
        P("ep", None, "tp"),
        P("ep", None, "tp"),
        P("ep", "tp", None),
    )
    out_specs = (P(("ep", "tp"), None), P("ep", "tp"))
    return jax.shard_map(body, mesh=mesh, in_specs=in_specs, out_specs=out_specs, check_vma=False)
```

profile of v0, /device:TPU:0, one launch (start us, length us, event | category | flops | bytes accessed | tf_op | source)
XLA Modules:
  0.0 162.9 jit_solution(18064462734204936463)
XLA Ops:
  7.2 0.9 copy.51
  8.1 0.1 eq.26
  8.3 0.1 reshape.190
  8.4 0.7 broadcast_multiply_fusion
  9.1 0.6 reduce-window.6
  9.7 0.2 slice_reduce_fusion
  9.9 0.1 copy.55
  10.0 0.1 mul.215
  10.2 0.1 fusion.59
  10.3 1.4 scatter_custom_fusion
  11.7 1.2 convert_reduce_fusion
  12.9 1.3 fusion.37
  14.3 1.4 fusion.39
  15.7 3.3 %gather_fusion = bf16[512,2048]{1,0:T(8,128)(2,1)} fusion(bf16[129,2048]{1,0:T(8,128)(2,1)S(1)} %concatenate.13, s32[1024]{0:T(1024)S(1)} %pad_clamp_fusion.1), kind=kCustom, calls=%fused_computation | custom fusion | bytes 4196352 | tf_op jit(solution)/shard_map/gather | solution.py:100
  19.1 6.5 %all-to-all-start = ((bf16[8,64,2048]{2,1,0:T(8,128)(2,1)}), bf16[8,64,2048]{2,1,0:T(8,128)(2,1)}, u32[]{:S(2)}, u32[]{:S(2)}) async-start(bf16[8,64,2048]{2,1,0:T(8,128)(2,1)} %bitcast.82), calls=%async_computation.1 | async-start | bytes 4194304 | tf_op jit(solution)/shard_map/all_to_all | solution.py:104
  25.7 0.1 fusion.42
  25.8 0.2 multiply_cosine_fusion
  26.1 1.5 convolution_convert_fusion.3
  27.6 47.2 %all-to-all-done = bf16[8,64,2048]{2,1,0:T(8,128)(2,1)} async-done(((bf16[8,64,2048]{2,1,0:T(8,128)(2,1)}), bf16[8,64,2048]{2,1,0:T(8,128)(2,1)}, u32[]{:S(2)}, u32[]{:S(2)}) %all-to-all-start) | async-done | bytes 2097184 | tf_op jit(solution)/shard_map/all_to_all | solution.py:104
  74.7 6.5 %fusion.5 = f32[512,1024]{1,0:T(8,128)} fusion(bf16[512,2048]{1,0:T(8,128)(2,1)} %bitcast.12, bf16[1,2048,1024]{2,1,0:T(8,128)(2,1)} %param.29), kind=kOutput, calls=%fused_computation.10 | convolution fusion | flops 2147483648 | bytes 8388608 | tf_op jit(solution)/shard_map/dot_general | solution.py:107
  81.2 10.6 %fusion.12 = bf16[2048,512]{0,1:T(8,128)(2,1)} fusion(bf16[1,1024,2048]{2,1,0:T(8,128)(2,1)} %param.31, f32[512,1024]{1,0:T(8,128)} %fusion.5, bf16[512,2048]{1,0:T(8,128)(2,1)} %bitcast.12, bf16[1,2048,1024]{2,1,0:T(8,128)(2,1)} %param.30), kind=kOutput, calls=%fused_computation.17 | convolution fusion | flops 4299161600 | bytes 14680064 | tf_op jit(solution)/shard_map/dot_general | solution.py:111
  91.9 0.4 reshape.186
  92.3 0.1 slice.21
  92.4 0.1 copy.60
  92.5 14.2 %all-gather = bf16[8,192,64]{1,2,0:T(8,128)(2,1)S(1)} all-gather(bf16[1,192,64]{1,2,0:T(8,128)(2,1)S(1)} %maximum_bitcast_fusion), channel_id=1, replica_groups=mesh['ep'=8,'tp'=4] {'ep'}, dimensions={0}, use_global_device_ids=true | all-gather | bytes 221184 | tf_op jit(solution)/shard_map/all_gather | solution.py:49
  106.7 0.1 copy.47
  106.9 0.2 reshape.223
  107.1 0.1 fusion.45
  107.3 0.1 fusion.47
  107.4 16.3 %all_gather.6 = bf16[1536,256]{1,0:T(8,128)(2,1)S(1)} all-gather(bf16[192,256]{1,0:T(8,128)(2,1)S(1)} %fusion.47), channel_id=1, replica_groups=mesh['ep'=8,'tp'=4] {'ep'}, dimensions={0}, use_global_device_ids=true | all-gather | bytes 884736 | tf_op jit(solution)/shard_map/all_gather | solution.py:48
  123.7 1.6 convolution_convert_fusion.1
  125.3 0.8 fusion.54
  126.1 0.1 slice-done
  126.2 0.9 fusion.65
  127.1 0.8 fusion.7
  127.9 0.2 copy-done.4
  128.0 0.6 convolution_convert_fusion
  128.7 0.9 fusion.34
  129.6 1.5 convolution_convert_fusion.2
  131.2 3.5 %all-to-all-start.1 = ((bf16[512,8,64]{0,2,1:T(8,128)(2,1)}), bf16[512,8,64]{0,2,1:T(8,128)(2,1)S(1)}, u32[]{:S(2)}, u32[]{:S(2)}) async-start(bf16[512,8,64]{0,2,1:T(8,128)(2,1)} %bitcast.86), calls=%async_computation.3 | async-start | bytes 1048576 | tf_op jit(solution)/shard_map/all_to_all | solution.py:119
  134.7 0.1 reduce_sum.83
  134.9 0.1 copy.54
  135.1 0.1 copy.56
  135.2 14.7 %all-to-all-done.1 = bf16[512,8,64]{0,2,1:T(8,128)(2,1)S(1)} async-done(((bf16[512,8,64]{0,2,1:T(8,128)(2,1)}), bf16[512,8,64]{0,2,1:T(8,128)(2,1)S(1)}, u32[]{:S(2)}, u32[]{:S(2)}) %all-to-all-start.1) | async-done | bytes 524320 | tf_op jit(solution)/shard_map/all_to_all | solution.py:119
  149.9 1.2 gather_fusion.1
  151.1 0.1 gather.11
  151.2 1.5 multiply_reduce_fusion
  152.7 3.4 %reduce-scatter.3.cloned.1.call-done = bf16[48,2048]{1,0:T(8,128)(2,1)} async-done(((bf16[192,2048]{1,0:T(8,128)(2,1)}), bf16[48,2048]{1,0:T(8,128)(2,1)}) %reduce-scatter.3.cloned.1.call-update) | async-done | bytes 196624 | tf_op jit(solution)/shard_map/reduce_scatter | solution.py:70
  (50 shorter events, 0.6 us)
Async XLA Ops:
  7.2 122.4 %copy-start = (bf16[512,2048]{1,0:T(8,128)(2,1)S(1)}, bf16[512,2048]{1,0:T(8,128)(2,1)}, u32[]{:S(2)}) copy-start(bf16[512,2048]{1,0:T(8,128)(2,1)} %param.24) | copy-start | bytes 6291460
  19.1 6.5 %copy-start.5 = (bf16[192,64]{0,1:T(8,128)(2,1)S(1)}, bf16[192,64]{0,1:T(8,128)(2,1)}, u32[]{:S(2)}) copy-start(bf16[192,64]{0,1:T(8,128)(2,1)} %param.18) | copy-start | bytes 73732
  19.1 6.6 %copy-start.2 = (bf16[192,512]{1,0:T(8,128)(2,1)S(1)}, bf16[192,512]{1,0:T(8,128)(2,1)}, u32[]{:S(2)}) copy-start(bf16[192,512]{1,0:T(8,128)(2,1)} %param.16) | copy-start | bytes 589828
  19.1 7.0 %copy-start.8 = (f32[512]{0:T(512)S(1)}, f32[512]{0:T(512)}, u32[]{:S(2)}) copy-start(f32[512]{0:T(512)} %param.19) | copy-start | bytes 6148
  19.1 55.6 %all-to-all-start = ((bf16[8,64,2048]{2,1,0:T(8,128)(2,1)}), bf16[8,64,2048]{2,1,0:T(8,128)(2,1)}, u32[]{:S(2)}, u32[]{:S(2)}) async-start(bf16[8,64,2048]{2,1,0:T(8,128)(2,1)} %bitcast.82), calls=%async_computation.1 | async-start | bytes 4194304 | tf_op jit(solution)/shard_map/all_to_all | solution.py:104
  25.6 105.6 %reduce-scatter.5.cloned.1.call-start = ((), (), s32[]{:S(2)}) async-start(), calls=%async_computation.5 | async-start | bytes 2621440 | tf_op jit(solution)/shard_map/reduce_scatter | solution.py:110
  91.8 15.3 %copy-start.3 = (bf16[192,256]{1,0:T(8,128)(2,1)S(1)}, bf16[192,256]{1,0:T(8,128)(2,1)}, u32[]{:S(2)}) copy-start(bf16[192,256]{1,0:T(8,128)(2,1)} %param.17) | copy-start | bytes 294916
  91.8 15.5 %copy-start.9 = (f32[256]{0:T(256)S(1)}, f32[256]{0:T(256)}, u32[]{:S(2)}) copy-start(f32[256]{0:T(256)} %param.20) | copy-start | bytes 3076
  91.8 64.3 %reduce-scatter.3.cloned.1.call-start = ((), (), s32[]{:S(2)}) async-start(), calls=%async_computation.4 | async-start | bytes 983040 | tf_op jit(solution)/shard_map/reduce_scatter | solution.py:70
  92.3 31.4 %copy-start.1 = (bf16[192,4,192]{2,1,0:T(4,128)(2,1)}, bf16[192,4,192]{2,1,0:T(4,128)(2,1)S(1)}, u32[]{:S(2)}) copy-start(bf16[192,4,192]{2,1,0:T(4,128)(2,1)S(1)} %reshape.186) | copy-start | bytes 884740
  125.3 0.9 slice-start
  127.1 1.0 copy-start.4
  129.6 5.3 %copy-start.6 = (s32[128,2]{0,1:T(2,128)S(1)}, s32[128,2]{0,1:T(2,128)}, u32[]{:S(2)}) copy-start(s32[128,2]{0,1:T(2,128)} %param.27) | copy-start | bytes 3076
  129.6 5.5 %copy-start.7 = (f32[128,2]{0,1:T(2,128)S(1)}, f32[128,2]{0,1:T(2,128)}, u32[]{:S(2)}) copy-start(f32[128,2]{0,1:T(2,128)} %param.28) | copy-start | bytes 3076
  131.2 18.8 %all-to-all-start.1 = ((bf16[512,8,64]{0,2,1:T(8,128)(2,1)}), bf16[512,8,64]{0,2,1:T(8,128)(2,1)S(1)}, u32[]{:S(2)}, u32[]{:S(2)}) async-start(bf16[512,8,64]{0,2,1:T(8,128)(2,1)} %bitcast.86), calls=%async_computation.3 | async-start | bytes 1048576 | tf_op jit(solution)/shard_map/all_to_all | solution.py:119
Sparse Core Ops, SparseCore 0:
  91.9 34.1 reduce-scatter.4
  131.3 24.7 reduce-scatter.2
where the time goes:
time: 164 us; the launch traced here: 163 us
  waiting for transfers between devices  65.3 us (40%)
  blocking collectives  30.5 us (19%)
  matrix products  24.9 us (15%)
  between operations  14.4 us (9%)
  starting transfers between devices  10.1 us (6%)
  local copies, waits for them, and re-layouts  9.44 us (6%)
  other arithmetic  8.38 us (5%)
    all_to_all x1, waiting for transfers between devices, experts(): lax.all_to_all(outgoing, 'ep', split_axis=0, concat_axis=0, tiled=True)  47.2 us
    all_gather x1, blocking collectives, mixer(): latent = lax.all_gather(kv_normed, 'ep', axis=0, tiled=True)  16.3 us
    all_to_all x1, waiting for transfers between devices, experts(): lax.all_to_all(summed.reshape(feature_count, expert_count, slots), 'ep',...  14.7 us
    all_gather x1, blocking collectives, mixer(): turned = lax.all_gather(key_turned, 'ep', axis=0, tiled=True)  14.2 us
    dot_general x1, matrix products, experts(): lax.dot_general(down_weight, hidden, (((0,), (1,)), ((), ())), preferred_...  10.6 us
    all_to_all x1, starting transfers between devices, experts(): lax.all_to_all(outgoing, 'ep', split_axis=0, concat_axis=0, tiled=True)  6.49 us
    dot_general x1, matrix products, experts(): gate = jnp.dot(arrived, gate_weight, preferred_element_type=jnp.float32)  6.48 us
    all_to_all x1, starting transfers between devices, experts(): lax.all_to_all(summed.reshape(feature_count, expert_count, slots), 'ep',...  3.5 us
  transfers between devices with their start and end apart: 4, of which 3 were waited for; matrix products, arithmetic and copies ran while one was open for 8% of the time, Pallas kernels for 0%

commit v1 on v0

--- a/solution.py
+++ b/solution.py
@@ -8,6 +8,20 @@
 VDIM = 128
 eps_norm = 1e-05
 rope_base = 10000.0
+
+
+def on_each_block(x, axis, dim, make, out_dim):
+    ways, here, step = (lax.axis_size(axis), lax.axis_index(axis), x.shape[dim])
+    earlier, later = ([], [])
+    going_up = going_down = x
+    for far in range(ways // 2 + 1):
+        earlier.append(make(going_up, (here - far) % ways * step))
+        if 0 < far < ways - ways // 2:
+            later.append(make(going_down, (here + far) % ways * step))
+        going_up = lax.ppermute(going_up, axis, [(d, (d + 1) % ways) for d in range(ways)])
+        going_down = lax.ppermute(going_down, axis, [(d, (d - 1) % ways) for d in range(ways)])
+    line = jnp.concatenate([*earlier[::-1], *later], axis=out_dim)
+    return jnp.roll(line, (here - ways // 2) * earlier[0].shape[out_dim], axis=out_dim)
 
 
 def rms_scale(values, gain):
@@ -46,7 +60,6 @@
     total = jnp.zeros((head_count, token_count), jnp.float32)
     summed = jnp.zeros((token_count, head_count, VDIM), jnp.float32)
     latent = lax.all_gather(kv_normed, "ep", axis=0, tiled=True)
-    turned = lax.all_gather(key_turned, "ep", axis=0, tiled=True)
     count = latent.shape[0]
     keys = jnp.dot(latent, w_key, preferred_element_type=jnp.float32).astype(jnp.bfloat16)
     keys = keys.reshape(count, head_count, NOPE)
@@ -54,7 +67,16 @@
     values = values.reshape(count, head_count, VDIM)
     scores = jnp.einsum("qhd,khd->hqk", q_pass, keys, preferred_element_type=jnp.float32)
     scores = (
-        scores + jnp.einsum("qhd,kd->hqk", q_turned, turned, preferred_element_type=jnp.float32)
+        scores
+        + on_each_block(
+            key_turned,
+            "ep",
+            0,
+            lambda shard, at: jnp.einsum(
+                "qhd,kd->hqk", q_turned, shard, preferred_element_type=jnp.float32
+            ),
+            2,
+        )
     ) * factor
     fresh = jnp.max(scores, -1)
     fade = jnp.exp(peak - fresh)

time: 164 us -> 183 us (1.12)
  waiting for transfers between devices: 65.3 us -> 20.7 us
  blocking collectives: 30.5 us -> 52.1 us
  matrix products: 24.9 us -> 40 us
  local copies, waits for them, and re-layouts: 9.44 us -> 22.7 us
  starting transfers between devices: 10.1 us -> 20.8 us
  other arithmetic: 8.38 us -> 11.3 us
    all_to_all x1, waiting for transfers between devices: 47.2 us -> 0.01 us  [experts(): lax.all_to_all(outgoing, 'ep', split_axis=0, concat_axis=0, tiled=True)]
    all_gather x1, blocking collectives: 16.3 us -> 52.1 us  [mixer(): latent = lax.all_gather(kv_normed, 'ep', axis=0, tiled=True)]
    all_gather x1 -> x0, blocking collectives: 14.2 us -> none  [mixer(): turned = lax.all_gather(key_turned, 'ep', axis=0, tiled=True)]
    concatenate x0 -> x1, local copies, waits for them, and re-layouts: none -> 12.7 us  [on_each_block(): jnp.roll(line, (here - ways // 2) * earlier[0].shape[out_dim], axis=out_dim)]
    ppermute x0 -> x7, starting transfers between devices: none -> 10.7 us  [the longest x3 9.79 us: on_each_block(): lax.ppermute(going_down, axis, [(d, (d - 1) % ways) for d in range(ways)])]
    dot_general x1 -> x8, matrix products: 0.81 us -> 10.3 us  [mixer(): jnp.einsum('qhd,kd->hqk', q_turned, shard, preferred_element_type=jnp.flo...]
    dot_general x1, matrix products: 0.87 us -> 4.44 us  [mixer(): jnp.einsum('qhd,khd->hqk', q_pass, keys, preferred_element_type=jnp.float32)]
    ppermute x0 -> x7, waiting for transfers between devices: none -> 2.72 us  [the longest x4 2.71 us: on_each_block(): lax.ppermute(going_up, axis, [(d, (d + 1) % ways) for d in range(ways)])]
  transfers between devices with their start and end apart: 4 -> 11, of which waited for: 3 -> 3; matrix products, arithmetic and copies ran while one was open for 8% -> 33% of each run, Pallas kernels for 0% -> 0%
where the time goes in v1:
time: 183 us; the launch traced here: 182 us
  blocking collectives  52.1 us (28%)
  matrix products  40 us (22%)
  local copies, waits for them, and re-layouts  22.7 us (12%)
  starting transfers between devices  20.8 us (11%)
  waiting for transfers between devices  20.7 us (11%)
  between operations  14.4 us (8%)
  other arithmetic  11.3 us (6%)
    all_gather x1, blocking collectives, mixer(): latent = lax.all_gather(kv_normed, 'ep', axis=0, tiled=True)  52.1 us
    all_to_all x1, waiting for transfers between devices, experts(): lax.all_to_all(summed.reshape(feature_count, expert_count, slots), 'ep',...  14.7 us
    concatenate x1, local copies, waits for them, and re-layouts, on_each_block(): jnp.roll(line, (here - ways // 2) * earlier[0].shape[out_dim], axis=out_dim)  12.7 us
    dot_general x1, matrix products, experts(): lax.dot_general(down_weight, hidden, (((0,), (1,)), ((), ())), preferred_...  10.5 us
    dot_general x8, matrix products, mixer(): jnp.einsum('qhd,kd->hqk', q_turned, shard, preferred_element_type=jnp.flo...  10.3 us
    ppermute x3, starting transfers between devices, on_each_block(): lax.ppermute(going_down, axis, [(d, (d - 1) % ways) for d in range(ways)])  9.79 us
    all_to_all x1, starting transfers between devices, experts(): lax.all_to_all(outgoing, 'ep', split_axis=0, concat_axis=0, tiled=True)  6.5 us
    dot_general x1, matrix products, experts(): gate = jnp.dot(arrived, gate_weight, preferred_element_type=jnp.float32)  6.45 us
  transfers between devices with their start and end apart: 11, of which 3 were waited for; matrix products, arithmetic and copies ran while one was open for 33% of the time, Pallas kernels for 0%

profile of v1, /device:TPU:0, one launch (start us, length us, event | category | flops | bytes accessed | tf_op | source)
XLA Modules:
  0.0 182.0 jit_solution(10498332403360430557)
XLA Ops:
  7.2 0.9 copy.38
  8.4 0.7 broadcast_multiply_fusion
  9.1 0.6 reduce-window.6
  9.7 0.2 slice_reduce_fusion
  10.3 1.4 scatter_custom_fusion
  11.7 1.2 convert_reduce_fusion
  12.9 1.3 fusion.36
  14.3 1.4 fusion.38
  15.7 3.3 %gather_fusion = bf16[512,2048]{1,0:T(8,128)(2,1)} fusion(bf16[129,2048]{1,0:T(8,128)(2,1)S(1)} %concatenate.20, s32[1024]{0:T(1024)S(1)} %pad_clamp_fusion.1), kind=kCustom, calls=%fused_computation | custom fusion | bytes 4196352 | tf_op jit(solution)/shard_map/gather | solution.py:122
  19.0 6.5 %all-to-all-start = ((bf16[8,64,2048]{2,1,0:T(8,128)(2,1)}), bf16[8,64,2048]{2,1,0:T(8,128)(2,1)}, u32[]{:S(2)}, u32[]{:S(2)}) async-start(bf16[8,64,2048]{2,1,0:T(8,128)(2,1)} %bitcast.113), calls=%async_computation.1 | async-start | bytes 4194304 | tf_op jit(solution)/shard_map/all_to_all | solution.py:126
  25.7 0.8 multiply_cosine_fusion
  26.5 0.6 pad_maximum_fusion.1
  27.1 0.5 collective-permute-start
  27.6 3.1 %collective-permute-start.4 = (bf16[192,64]{0,1:T(8,128)(2,1)}, bf16[192,64]{0,1:T(8,128)(2,1)}, u32[]{:S(2)}, u32[]{:S(2)}) collective-permute-start(bf16[192,64]{0,1:T(8,128)(2,1)} %pad_maximum_fusion.1), channel_id=1, source_target_pairs={{0,28},{4,0},{8,4},{12,8},{16,12},{20,16},{24,20},{28,24},{1,29},{... | collective-permute-start | bytes 73736 | tf_op jit(solution)/shard_map/ppermute | solution.py:22
  30.8 0.4 convolution_convert_fusion.3
  31.2 0.4 reshape.186
  31.6 0.1 copy.47
  31.8 0.7 convert_element_type.92
  32.7 52.1 %all_gather.3 = bf16[1536,256]{1,0:T(8,128)(2,1)S(1)} all-gather(bf16[192,256]{1,0:T(8,128)(2,1)S(1)} %fusion.46), channel_id=1, replica_groups=mesh['ep'=8,'tp'=4] {'ep'}, dimensions={0}, use_global_device_ids=true | all-gather | bytes 884736 | tf_op jit(solution)/shard_map/all_gather | solution.py:62
  84.8 2.8 %convolution_convert_fusion.1 = bf16[1536,512]{0,1:T(8,128)(2,1)} fusion(bf16[1536,256]{1,0:T(8,128)(2,1)S(1)} %all_gather.3, bf16[256,512]{1,0:T(8,128)(2,1)} %param.22), kind=kOutput, calls=%fused_computation.15 | convolution fusion | flops 403439616 | bytes 2621440 | tf_op jit(solution)/shard_map/dot_general | solution.py:64
  87.6 6.4 %fusion.4 = f32[512,1024]{1,0:T(8,128)} fusion(bf16[512,2048]{1,0:T(8,128)(2,1)} %bitcast.26, bf16[1,2048,1024]{2,1,0:T(8,128)(2,1)} %param.29), kind=kOutput, calls=%fused_computation.9 | convolution fusion | flops 2147483648 | bytes 8388608 | tf_op jit(solution)/shard_map/dot_general | solution.py:129
  94.0 10.5 %fusion.11 = bf16[2048,512]{0,1:T(8,128)(2,1)} fusion(bf16[1,1024,2048]{2,1,0:T(8,128)(2,1)} %param.31, f32[512,1024]{1,0:T(8,128)} %fusion.4, bf16[512,2048]{1,0:T(8,128)(2,1)} %bitcast.26, bf16[1,2048,1024]{2,1,0:T(8,128)(2,1)} %param.30), kind=kOutput, calls=%fused_computation.16 | convolution fusion | flops 4299161600 | bytes 14680064 | tf_op jit(solution)/shard_map/dot_general | solution.py:133
  104.6 0.7 copy-done.6
  105.3 1.0 subtract_convert_fusion
  106.3 2.7 %convolution_convert_fusion = bf16[1536,512]{0,1:T(8,128)(2,1)} fusion(bf16[1536,256]{1,0:T(8,128)(2,1)S(1)} %all_gather.3, bf16[256,512]{1,0:T(8,128)(2,1)} %param.23), kind=kOutput, calls=%fused_computation.14 | convolution fusion | flops 403439616 | bytes 2621440 | tf_op jit(solution)/shard_map/dot_general | solution.py:66
  109.1 0.3 convolution_bitcast_fusion.3
  109.4 0.4 collective-permute-start.1
  109.8 3.2 %collective-permute-start.5 = (bf16[192,64]{0,1:T(8,128)(2,1)}, bf16[192,64]{0,1:T(8,128)(2,1)S(1)}, u32[]{:S(2)}, u32[]{:S(2)}) collective-permute-start(bf16[192,64]{0,1:T(8,128)(2,1)} %collective-permute-done.4), channel_id=1, source_target_pairs={{0,28},{4,0},{8,4},{12,8},{16,12},{20,16},{24,20},{28,24},{1,29},{... | collective-permute-start | bytes 73736 | tf_op jit(solution)/shard_map/ppermute | solution.py:22
  113.0 2.0 %convolution_bitcast_fusion.2 = f32[4,192,192]{2,1,0:T(8,128)} fusion(bf16[192,64]{0,1:T(8,128)(2,1)} %collective-permute-done.4, bf16[192,4,32]{0,2,1:T(8,128)(2,1)S(1)} %get-tuple-element.3, bf16[192,4,32]{0,2,1:T(8,128)(2,1)S(1)} %get-tuple-element.2), kind=kOutput, calls=%fused_computation.25 | convolution fusion | flops 19070976 | bytes 712704 | tf_op jit(solution)/shard_map/qhd,kd->hqk/dot_general | solution.py:75
  115.0 2.0 %convolution_bitcast_fusion.4 = f32[4,192,192]{2,1,0:T(8,128)} fusion(bf16[192,64]{0,1:T(8,128)(2,1)} %collective-permute-done, bf16[192,4,32]{0,2,1:T(8,128)(2,1)S(1)} %get-tuple-element.3, bf16[192,4,32]{0,2,1:T(8,128)(2,1)S(1)} %get-tuple-element.2), kind=kOutput, calls=%fused_computation.27 | convolution fusion | flops 19070976 | bytes 712704 | tf_op jit(solution)/shard_map/qhd,kd->hqk/dot_general | solution.py:75
  117.0 3.5 %collective-permute-start.6 = (bf16[192,64]{0,1:T(8,128)(2,1)S(1)}, bf16[192,64]{0,1:T(8,128)(2,1)S(1)}, u32[]{:S(2)}, u32[]{:S(2)}) collective-permute-start(bf16[192,64]{0,1:T(8,128)(2,1)S(1)} %collective-permute-done.5), channel_id=1, source_target_pairs={{0,28},{4,0},{8,4},{12,8},{16,12},{20,16},{24,20},{28,24},{1,29},{... | collective-permute-start | bytes 73736 | tf_op jit(solution)/shard_map/ppermute | solution.py:22
  120.5 1.2 convolution_bitcast_fusion.1
  121.7 1.2 convolution_bitcast_fusion.5
  123.0 1.2 convolution_bitcast_fusion.6
  124.2 1.2 convolution_bitcast_fusion
  125.4 2.7 %collective-permute-done.3 = bf16[192,64]{0,1:T(8,128)(2,1)S(1)} collective-permute-done((bf16[192,64]{0,1:T(8,128)(2,1)S(1)}, bf16[192,64]{0,1:T(8,128)(2,1)S(1)}, u32[]{:S(2)}, u32[]{:S(2)}) %collective-permute-start.3) | collective-permute-done | bytes 24608 | tf_op jit(solution)/shard_map/ppermute | solution.py:21
  128.1 1.2 convolution_bitcast_fusion.7
  129.3 12.7 %concatenate.19 = f32[4,192,3072]{2,1,0:T(8,128)} concatenate(f32[4,192,192]{2,1,0:T(8,128)} %convolution_bitcast_fusion.7, f32[4,192,192]{2,1,0:T(8,128)} %convolution_bitcast_fusion.6, f32[4,192,192]{2,1,0:T(8,128)} %convolution_bitcast_fusion.5, f32[4,192,192]{2,1,0:T(8,128)} %convolution_bitcast_fusion.4, f32[4,192,192]{2,1,0:T(8,128)S(1)} %convolution_bitcast_fusion.3, ...), dimensions={2} | concatenate | bytes 18874368 | tf_op jit(solution)/shard_map/jit(_roll_dynamic)/concatenate | solution.py:24
  142.0 4.4 %fusion.70 = (f32[4,192]{1,0:T(4,128)S(1)}, f32[4,192,1536]{2,1,0:T(8,128)S(1)}) fusion(f32[4,192,3072]{2,1,0:T(8,128)} %concatenate.19, s32[]{:T(128)S(6)} %select_n.44, bf16[1536,4,128]{0,2,1:T(8,128)(2,1)} %bitcast.114, bf16[192,4,128]{2,1,0:T(4,128)(2,1)S(1)} %slice-done), kind=kOutput, calls=%fused_computation.107 | convolution fusion | flops 305528064 | bytes 11209732 | tf_op jit(solution)/shard_map/qhd,khd->hqk/dot_general | solution.py:68
  146.5 0.8 fusion.6
  147.3 0.6 copy-done.1
  147.9 0.9 fusion.33
  148.8 1.5 convolution_convert_fusion.2
  150.3 3.5 %all-to-all-start.1 = ((bf16[512,8,64]{0,2,1:T(8,128)(2,1)}), bf16[512,8,64]{0,2,1:T(8,128)(2,1)S(1)}, u32[]{:S(2)}, u32[]{:S(2)}) async-start(bf16[512,8,64]{0,2,1:T(8,128)(2,1)} %bitcast.117), calls=%async_computation.3 | async-start | bytes 1048576 | tf_op jit(solution)/shard_map/all_to_all | solution.py:141
  154.4 14.7 %all-to-all-done.1 = bf16[512,8,64]{0,2,1:T(8,128)(2,1)S(1)} async-done(((bf16[512,8,64]{0,2,1:T(8,128)(2,1)}), bf16[512,8,64]{0,2,1:T(8,128)(2,1)S(1)}, u32[]{:S(2)}, u32[]{:S(2)}) %all-to-all-start.1) | async-done | bytes 524320 | tf_op jit(solution)/shard_map/all_to_all | solution.py:141
  169.1 1.2 gather_fusion.1
  170.4 1.5 multiply_reduce_fusion
  171.9 3.3 %reduce-scatter.3.cloned.1.call-done = bf16[48,2048]{1,0:T(8,128)(2,1)} async-done(((bf16[192,2048]{1,0:T(8,128)(2,1)}), bf16[48,2048]{1,0:T(8,128)(2,1)}) %reduce-scatter.3.cloned.1.call-update) | async-done | bytes 196624 | tf_op jit(solution)/shard_map/reduce_scatter | solution.py:92
  (75 shorter events, 2.0 us)
Async XLA Ops:
  7.2 141.6 %copy-start = (bf16[512,2048]{1,0:T(8,128)(2,1)S(1)}, bf16[512,2048]{1,0:T(8,128)(2,1)}, u32[]{:S(2)}) copy-start(bf16[512,2048]{1,0:T(8,128)(2,1)} %param.24) | copy-start | bytes 6291460
  19.0 6.6 %copy-start.8 = (bf16[192,64]{0,1:T(8,128)(2,1)S(1)}, bf16[192,64]{0,1:T(8,128)(2,1)}, u32[]{:S(2)}) copy-start(bf16[192,64]{0,1:T(8,128)(2,1)} %param.18) | copy-start | bytes 73732
  19.0 11.6 %copy-start.4 = (bf16[192,512]{1,0:T(8,128)(2,1)S(1)}, bf16[192,512]{1,0:T(8,128)(2,1)}, u32[]{:S(2)}) copy-start(bf16[192,512]{1,0:T(8,128)(2,1)} %param.16) | copy-start | bytes 589828
  19.0 11.8 %copy-start.3 = (bf16[512,768]{1,0:T(8,128)(2,1)S(1)}, bf16[512,768]{1,0:T(8,128)(2,1)}, u32[]{:S(2)}) copy-start(bf16[512,768]{1,0:T(8,128)(2,1)} %param.21) | copy-start | bytes 2359300
  19.0 11.8 %copy-start.11 = (f32[512]{0:T(512)S(1)}, f32[512]{0:T(512)}, u32[]{:S(2)}) copy-start(f32[512]{0:T(512)} %param.19) | copy-start | bytes 6148
  19.0 68.5 %all-to-all-start = ((bf16[8,64,2048]{2,1,0:T(8,128)(2,1)}), bf16[8,64,2048]{2,1,0:T(8,128)(2,1)}, u32[]{:S(2)}, u32[]{:S(2)}) async-start(bf16[8,64,2048]{2,1,0:T(8,128)(2,1)} %bitcast.113), calls=%async_computation.1 | async-start | bytes 4194304 | tf_op jit(solution)/shard_map/all_to_all | solution.py:126
  25.5 7.0 %copy-start.5 = (bf16[192,256]{1,0:T(8,128)(2,1)S(1)}, bf16[192,256]{1,0:T(8,128)(2,1)}, u32[]{:S(2)}) copy-start(bf16[192,256]{1,0:T(8,128)(2,1)} %param.17) | copy-start | bytes 294916
  25.5 7.1 %copy-start.12 = (f32[256]{0:T(256)S(1)}, f32[256]{0:T(256)}, u32[]{:S(2)}) copy-start(f32[256]{0:T(256)} %param.20) | copy-start | bytes 3076
  25.6 124.8 %reduce-scatter.5.cloned.1.call-start = ((), (), s32[]{:S(2)}) async-start(), calls=%async_computation.5 | async-start | bytes 2621440 | tf_op jit(solution)/shard_map/reduce_scatter | solution.py:132
  27.1 82.3 %collective-permute-start = (bf16[192,64]{0,1:T(8,128)(2,1)}, bf16[192,64]{0,1:T(8,128)(2,1)}, u32[]{:S(2)}, u32[]{:S(2)}) collective-permute-start(bf16[192,64]{0,1:T(8,128)(2,1)} %pad_maximum_fusion.1), channel_id=1, source_target_pairs={{0,4},{4,8},{8,12},{12,16},{16,20},{20,24},{24,28},{28,0},{1,5},{5... | collective-permute-start | bytes 73736 | tf_op jit(solution)/shard_map/ppermute | solution.py:21
  27.6 82.2 %collective-permute-start.4 = (bf16[192,64]{0,1:T(8,128)(2,1)}, bf16[192,64]{0,1:T(8,128)(2,1)}, u32[]{:S(2)}, u32[]{:S(2)}) collective-permute-start(bf16[192,64]{0,1:T(8,128)(2,1)} %pad_maximum_fusion.1), channel_id=1, source_target_pairs={{0,28},{4,0},{8,4},{12,8},{16,12},{20,16},{24,20},{28,24},{1,29},{... | collective-permute-start | bytes 73736 | tf_op jit(solution)/shard_map/ppermute | solution.py:22
  31.5 77.9 %copy-start.2 = (bf16[192,4,192]{2,1,0:T(4,128)(2,1)}, bf16[192,4,192]{2,1,0:T(4,128)(2,1)S(1)}, u32[]{:S(2)}) copy-start(bf16[192,4,192]{2,1,0:T(4,128)(2,1)S(1)} %reshape.186) | copy-start | bytes 884740
  104.6 0.8 copy-start.6
  104.6 0.8 copy-start.7
  104.6 70.6 %reduce-scatter.3.cloned.1.call-start = ((), (), s32[]{:S(2)}) async-start(), calls=%async_computation.4 | async-start | bytes 983040 | tf_op jit(solution)/shard_map/reduce_scatter | solution.py:92
  109.4 7.6 %collective-permute-start.1 = (bf16[192,64]{0,1:T(8,128)(2,1)}, bf16[192,64]{0,1:T(8,128)(2,1)S(1)}, u32[]{:S(2)}, u32[]{:S(2)}) collective-permute-start(bf16[192,64]{0,1:T(8,128)(2,1)} %collective-permute-done), channel_id=1, source_target_pairs={{0,4},{4,8},{8,12},{12,16},{16,20},{20,24},{24,28},{28,0},{1,5},{5... | collective-permute-start | bytes 73736 | tf_op jit(solution)/shard_map/ppermute | solution.py:21
  109.8 7.2 %collective-permute-start.5 = (bf16[192,64]{0,1:T(8,128)(2,1)}, bf16[192,64]{0,1:T(8,128)(2,1)S(1)}, u32[]{:S(2)}, u32[]{:S(2)}) collective-permute-start(bf16[192,64]{0,1:T(8,128)(2,1)} %collective-permute-done.4), channel_id=1, source_target_pairs={{0,28},{4,0},{8,4},{12,8},{16,12},{20,16},{24,20},{28,24},{1,29},{... | collective-permute-start | bytes 73736 | tf_op jit(solution)/shard_map/ppermute | solution.py:22
  117.0 6.0 %collective-permute-start.2 = (bf16[192,64]{0,1:T(8,128)(2,1)S(1)}, bf16[192,64]{0,1:T(8,128)(2,1)S(1)}, u32[]{:S(2)}, u32[]{:S(2)}) collective-permute-start(bf16[192,64]{0,1:T(8,128)(2,1)S(1)} %collective-permute-done.1), channel_id=1, source_target_pairs={{0,4},{4,8},{8,12},{12,16},{16,20},{20,24},{24,28},{28,0},{1,5},{5... | collective-permute-start | bytes 73736 | tf_op jit(solution)/shard_map/ppermute | solution.py:21
  117.0 7.2 %collective-permute-start.6 = (bf16[192,64]{0,1:T(8,128)(2,1)S(1)}, bf16[192,64]{0,1:T(8,128)(2,1)S(1)}, u32[]{:S(2)}, u32[]{:S(2)}) collective-permute-start(bf16[192,64]{0,1:T(8,128)(2,1)S(1)} %collective-permute-done.5), channel_id=1, source_target_pairs={{0,28},{4,0},{8,4},{12,8},{16,12},{20,16},{24,20},{28,24},{1,29},{... | collective-permute-start | bytes 73736 | tf_op jit(solution)/shard_map/ppermute | solution.py:22
  123.0 5.1 %collective-permute-start.3 = (bf16[192,64]{0,1:T(8,128)(2,1)S(1)}, bf16[192,64]{0,1:T(8,128)(2,1)S(1)}, u32[]{:S(2)}, u32[]{:S(2)}) collective-permute-start(bf16[192,64]{0,1:T(8,128)(2,1)S(1)} %collective-permute-done.2), channel_id=1, source_target_pairs={{0,4},{4,8},{8,12},{12,16},{16,20},{20,24},{24,28},{28,0},{1,5},{5... | collective-permute-start | bytes 73736 | tf_op jit(solution)/shard_map/ppermute | solution.py:21
  129.3 12.7 %slice-start = ((bf16[192,4,192]{2,1,0:T(4,128)(2,1)}), bf16[192,4,128]{2,1,0:T(4,128)(2,1)S(1)}, s32[]{:S(2)}) async-start(bf16[192,4,192]{2,1,0:T(4,128)(2,1)} %copy-done.2), calls=%async_computation.6 | async-start | bytes 393216 | tf_op jit(solution)/shard_map/slice | solution.py:54
  146.5 1.4 copy-start.1
  148.8 5.3 %copy-start.9 = (s32[128,2]{0,1:T(2,128)S(1)}, s32[128,2]{0,1:T(2,128)}, u32[]{:S(2)}) copy-start(s32[128,2]{0,1:T(2,128)} %param.27) | copy-start | bytes 3076
  148.8 5.4 %copy-start.10 = (f32[128,2]{0,1:T(2,128)S(1)}, f32[128,2]{0,1:T(2,128)}, u32[]{:S(2)}) copy-start(f32[128,2]{0,1:T(2,128)} %param.28) | copy-start | bytes 3076
  150.3 18.8 %all-to-all-start.1 = ((bf16[512,8,64]{0,2,1:T(8,128)(2,1)}), bf16[512,8,64]{0,2,1:T(8,128)(2,1)S(1)}, u32[]{:S(2)}, u32[]{:S(2)}) async-start(bf16[512,8,64]{0,2,1:T(8,128)(2,1)} %bitcast.117), calls=%async_computation.3 | async-start | bytes 1048576 | tf_op jit(solution)/shard_map/all_to_all | solution.py:141
Sparse Core Ops, SparseCore 0:
  104.7 35.5 reduce-scatter.4
  150.4 24.6 reduce-scatter.2
